TPU v7x, 32 devices: a whole 2x2x4 slice. The times are simulated.
32 devices in a mesh: sp: 4 (over z), fs: 4 (over y, core), tp: 2 (over x).
Axes of the slice: x: 2, y: 2, z: 4, core: 2. Of those that a mesh axis runs over, the one named last changes fastest.
Arguments:
- tokens: bfloat16 [8, 2048, 2048], P('fs', ('sp', 'tp')), may hold values from -6 to 6
- norm_gain: float32 [2048], replicated, may hold values from 0.1 to 1.9
- w_pool_in: bfloat16 [2048, 1024], P('fs', 'tp'), may hold values from -0.125 to 0.125
- pool_mix: bfloat16 [8, 128, 128], replicated, may hold values from -0.5 to 0.5
- pool_scale: float32 [1024], replicated, may hold values from 0.1 to 1.9
- w_query: bfloat16 [2048, 1024], P('fs', 'tp'), may hold values from -0.13258252 to 0.13258252
- w_key: bfloat16 [2048, 1024], P('fs', 'tp'), may hold values from -0.508233 to 0.508233
- w_value: bfloat16 [2048, 1024], P('fs', 'tp'), may hold values from -0.125 to 0.125
- gate_cache: float32 [8, 8, 2048], P('fs', 'tp'), may hold values from -258 to 0, as said below
- w_out_pool: bfloat16 [1024, 2048], P('tp', 'fs'), may hold values from -0.125 to 0.125
- w_out_attn: bfloat16 [1024, 2048], P('tp', 'fs'), may hold values from -0.75 to 0.75
Outputs:
- mixed: bfloat16 [8, 2048, 2048], P('fs', ('sp', 'tp'))
Inputs may be any that keep to these rules, and one draw needn't show every extreme that they name: `gate_cache`: each head's values never rise along the positions.
All inputs are finite; a program needn't handle non-finite values.
Results may differ from a plain program's by a relative error of at most 0.014.
Values may be sent and summed in bfloat16 or wider, within the bound.
A program may use at most 128 MiB of HBM per device.

v0:
```python
import jax
import jax.numpy as jnp
from jax import lax
from jax.experimental import pallas as pl
from jax.experimental.pallas import tpu as pltpu
from jax.sharding import PartitionSpec as P

HEAD_DIM = 128
GROUP_WIDTH = 128


norm_eps = 1e-06
widest = 16
masked_score = -1e30


def shifted(x, axis, by):
    length = lax.axis_size(axis)
    pairs = [(i, i + by) for i in range(length) if 0 <= i + by < length]
    return lax.ppermute(x, axis, pairs)


def window_sums(extended):
    outcome = []
    current = extended
    offset = 1
    for doubling in range(4):
        padding = jnp.zeros((offset, extended.shape[1]), jnp.float32)
        current = current + jnp.concatenate([padding, current[:-offset]], axis=0)
        offset = offset * 2
        outcome.append(current[widest - 1 :])
    return outcome


def pool_branch(projected, border, first_group, first_position, mixing, scaling):
    row_count = projected.shape[0]
    channels = projected.shape[1]
    widened = projected.astype(jnp.float32)
    totals = window_sums(jnp.concatenate([border.astype(jnp.float32), widened], axis=0))
    token_positions = first_position + jnp.arange(row_count)
    window_index = (first_group + jnp.arange(channels) // GROUP_WIDTH) % 4
    averaged = jnp.zeros((row_count, channels), jnp.float32)
    for doubling in range(4):
        counted = jnp.minimum(token_positions + 1, 2 ** (doubling + 1)).astype(jnp.float32)
        picked = (window_index == doubling).astype(jnp.float32)
        averaged = averaged + picked[None, :] * totals[doubling] / counted[:, None]
    departure = (averaged - widened).astype(jnp.bfloat16)
    group_count = channels // GROUP_WIDTH
    mixed_rows = jnp.einsum(
        "tgc,gcd->tgd",
        departure.reshape(row_count, group_count, GROUP_WIDTH),
        mixing,
        preferred_element_type=jnp.float32,
    )
    return (mixed_rows.reshape(row_count, channels) * scaling[None, :]).astype(jnp.bfloat16)


def general_device(
    tokens,
    norm_gain,
    w_pool_in,
    pool_mix,
    pool_scale,
    w_query,
    w_key,
    w_value,
    gate_cache,
    w_out_pool,
    w_out_attn,
):
    tp_index = lax.axis_index("tp")
    tp_count = lax.axis_size("tp")
    seq_count = tokens.shape[0]
    own_count = tokens.shape[1]
    token_count = own_count * tp_count
    first_position = lax.axis_index("sp") * token_count
    own_rows = tokens.astype(jnp.float32)
    normed = (
        own_rows
        * lax.rsqrt(jnp.mean(own_rows * own_rows, axis=-1, keepdims=True) + norm_eps)
        * norm_gain[None, None, :]
    ).astype(jnp.bfloat16)
    pool_full, query_full, key_full, value_full, out_pool_full, out_attn_full = (
        lax.all_gather(w_pool_in, "fs", axis=0, tiled=True),
        lax.all_gather(w_query, "fs", axis=0, tiled=True),
        lax.all_gather(w_key, "fs", axis=0, tiled=True),
        lax.all_gather(w_value, "fs", axis=0, tiled=True),
        lax.all_gather(w_out_pool, "fs", axis=1, tiled=True),
        lax.all_gather(w_out_attn, "fs", axis=1, tiled=True),
    )
    pool_cols = w_pool_in.shape[1]
    attn_cols = w_query.shape[1]
    shard_rows = lax.all_gather(normed, "tp", axis=1, tiled=True)
    projected = jnp.concatenate(
        [
            jnp.dot(shard_rows, pool_full, preferred_element_type=jnp.float32).astype(jnp.bfloat16),
            jnp.dot(shard_rows, query_full, preferred_element_type=jnp.float32).astype(
                jnp.bfloat16
            ),
            jnp.dot(shard_rows, key_full, preferred_element_type=jnp.float32).astype(jnp.bfloat16),
            jnp.dot(shard_rows, value_full, preferred_element_type=jnp.float32).astype(
                jnp.bfloat16
            ),
        ],
        axis=2,
    )
    pool_in = projected[:, :, :pool_cols]
    query_proj = projected[:, :, pool_cols : pool_cols + attn_cols]
    key_proj = projected[:, :, pool_cols + attn_cols : pool_cols + 2 * attn_cols]
    value_proj = projected[:, :, pool_cols + 2 * attn_cols :]
    group_local = pool_cols // GROUP_WIDTH
    mixing = lax.dynamic_slice_in_dim(pool_mix, tp_index * group_local, group_local, 0)
    scaling = lax.dynamic_slice_in_dim(pool_scale, tp_index * pool_cols, pool_cols, 0)
    borders = shifted(pool_in[:, token_count - (widest - 1) :], "sp", 1)
    pool_out = jnp.stack(
        [
            pool_branch(
                pool_in[member],
                borders[member],
                tp_index * group_local,
                first_position,
                mixing,
                scaling,
            )
            for member in range(seq_count)
        ],
        axis=0,
    )
    head_count = attn_cols // HEAD_DIM
    query_heads = query_proj.reshape(seq_count, token_count, head_count, HEAD_DIM)
    query_gates = jnp.transpose(
        lax.dynamic_slice_in_dim(gate_cache, first_position, token_count, 2), (0, 2, 1)
    )
    query_positions = first_position + jnp.arange(token_count)
    last_position = first_position + token_count - 1
    score_scale = HEAD_DIM ** (-0.5)
    start_state = (
        jnp.full((seq_count, token_count, head_count), masked_score, jnp.float32),
        jnp.zeros((seq_count, token_count, head_count), jnp.float32),
        jnp.zeros((seq_count, token_count, head_count, HEAD_DIM), jnp.float32),
    )
    key_shard = lax.all_gather(key_proj, "sp", axis=1, tiled=True)
    value_shard = lax.all_gather(value_proj, "sp", axis=1, tiled=True)
    key_total = key_shard.shape[1]
    block_rows = 512

    def one_block(block_state, block_index):
        key_start = block_index * block_rows

        def compute(inner_state):
            running_top, running_sum, running_out = inner_state
            key_block = lax.dynamic_slice_in_dim(key_shard, block_index * block_rows, block_rows, 1)
            value_block = lax.dynamic_slice_in_dim(
                value_shard, block_index * block_rows, block_rows, 1
            )
            key_block = key_block.reshape(seq_count, block_rows, head_count, HEAD_DIM)
            value_block = value_block.reshape(seq_count, block_rows, head_count, HEAD_DIM)
            key_gates = lax.dynamic_slice_in_dim(gate_cache, key_start, block_rows, 2)
            scores = (
                jnp.einsum(
                    "sqhd,skhd->sqhk", query_heads, key_block, preferred_element_type=jnp.float32
                )
                * score_scale
            )
            scores = scores + query_gates[:, :, :, None] - key_gates[:, None, :, :]
            allowed = ((key_start + jnp.arange(block_rows))[None, :] <= query_positions[:, None])[
                None, :, None, :
            ]
            scores = jnp.where(allowed, scores, masked_score)
            new_top = jnp.maximum(running_top, jnp.max(scores, axis=3))
            weights = jnp.where(allowed, jnp.exp(scores - new_top[:, :, :, None]), 0.0)
            shrink = jnp.exp(running_top - new_top)
            running_sum = running_sum * shrink + jnp.sum(weights, axis=3)
            running_out = running_out * shrink[:, :, :, None] + jnp.einsum(
                "sqhk,skhd->sqhd",
                weights.astype(jnp.bfloat16),
                value_block,
                preferred_element_type=jnp.float32,
            )
            return (new_top, running_sum, running_out)

        def unchanged(inner_state):
            return inner_state

        return (lax.cond(key_start <= last_position, compute, unchanged, block_state), None)

    result, unused = lax.scan(one_block, start_state, jnp.arange(key_total // block_rows))
    final_top, final_sum, final_out = result
    attn_out = (
        (final_out / final_sum[:, :, :, None])
        .astype(jnp.bfloat16)
        .reshape(seq_count, token_count, attn_cols)
    )
    pool_flat = jnp.transpose(
        pool_out.reshape(seq_count, tp_count, own_count, pool_cols), (1, 0, 2, 3)
    ).reshape(tp_count * seq_count * own_count, pool_cols)
    attn_flat = jnp.transpose(
        attn_out.reshape(seq_count, tp_count, own_count, attn_cols), (1, 0, 2, 3)
    ).reshape(tp_count * seq_count * own_count, attn_cols)
    summed = lax.psum_scatter(
        (
            jnp.dot(pool_flat, out_pool_full, preferred_element_type=jnp.float32)
            + jnp.dot(attn_flat, out_attn_full, preferred_element_type=jnp.float32)
        ).astype(jnp.bfloat16),
        "tp",
        scatter_dimension=0,
        tiled=True,
    ).astype(jnp.float32)
    return summed.astype(jnp.bfloat16).reshape(seq_count, own_count, summed.shape[1])


log2_e = 1.4426950408889634
MESH = pl.DeviceIdType.MESH
KEY, VALUE, QUERY, POOL = 0, 1, 2, 3


def layer_kernel(
    tokens,
    gain,
    w_pool,
    mix,
    scale,
    w_query,
    w_key,
    w_value,
    gates,
    w_out_pool,
    w_out_attn,
    out,
    w_in,
    w_out,
    rows_ref,
    stage,
    heads,
    extended,
    border_out,
    border_in,
    pool_tmp,
    pool_rows,
    attn_own,
    attn_rows,
    out_stage,
    local_sem,
    send_sem,
    recv_sem,
    attn_send,
    attn_recv,
):
    z = lax.axis_index("sp")
    f = lax.axis_index("fs")
    x = lax.axis_index("tp")
    seqs, half, width = tokens.shape
    block = 2 * half
    depth, cols = w_key.shape
    other_x = 1 - x
    sibling = f + 1 - 2 * lax.rem(f, 2)
    across = lax.rem(f + 2, 4)
    z_count = stage.shape[3]

    def z_at(by):
        return lax.rem(z + by, z_count)

    barrier = pltpu.get_barrier_semaphore()
    peers = [{"tp": other_x}, {"fs": sibling}, {"fs": across}]
    for by in range(1, z_count):
        peers.append({"sp": z_at(by)})
        peers.append({"sp": z_at(by), "tp": other_x})
    for peer in peers:
        pl.semaphore_signal(barrier, inc=1, device_id=peer, device_id_type=MESH)
    pl.semaphore_wait(barrier, len(peers))

    numbers = iter(range(send_sem.shape[0]))

    def remote(source, target, peer):
        number = next(numbers)
        return pltpu.make_async_remote_copy(
            src_ref=source,
            dst_ref=target,
            send_sem=send_sem.at[number],
            recv_sem=recv_sem.at[number],
            device_id=peer,
            device_id_type=MESH,
        )

    local_numbers = iter(range(local_sem.shape[0]))

    def local(source, target):
        return pltpu.make_async_copy(source, target, local_sem.at[next(local_numbers)])

    def in_slot(kind, owner):
        return w_in.at[kind, pl.ds(pl.multiple_of(owner * depth, depth), depth)]

    def out_slot(kind, owner_x, owner_f):
        return w_out.at[
            kind,
            pl.ds(pl.multiple_of(owner_x * cols, cols), cols),
            pl.ds(pl.multiple_of(owner_f * depth, depth), depth),
        ]

    w_own = (w_key, w_value, w_query, w_pool)
    out_own = (w_out_pool, w_out_attn)
    kinds = range(4)

    tok_x = [remote(tokens.at[s], rows_ref.at[s, 1], {"tp": other_x}) for s in range(seqs)]
    in_y = [remote(w_own[k], in_slot(k, f), {"fs": across}) for k in kinds]
    in_sib = [remote(w_own[k], in_slot(k, f), {"fs": sibling}) for k in kinds]
    in_corner = [remote(in_slot(k, across), in_slot(k, across), {"fs": sibling}) for k in kinds]
    out_x = [remote(out_own[k], out_slot(k, x, f), {"tp": other_x}) for k in range(2)]
    out_y = [remote(out_own[k], out_slot(k, x, f), {"fs": across}) for k in range(2)]
    out_sib = [remote(out_own[k], out_slot(k, x, f), {"fs": sibling}) for k in range(2)]

    def forwarded(owner_x, owner_f, peer):
        return [
            remote(out_slot(k, owner_x, owner_f), out_slot(k, owner_x, owner_f), peer)
            for k in range(2)
        ]

    out_xy = forwarded(other_x, f, {"fs": across})
    out_xs = forwarded(other_x, f, {"fs": sibling})
    out_ys = forwarded(x, across, {"fs": sibling})
    out_xys = forwarded(other_x, across, {"fs": sibling})
    tok_local = [local(tokens.at[s], rows_ref.at[s, 0]) for s in range(seqs)]
    in_local = [local(w_own[k], in_slot(k, f)) for k in kinds]
    out_local = [local(out_own[k], out_slot(k, x, f)) for k in range(2)]

    def start(copies):
        for copy in copies:
            copy.start()

    def arrive(copies):
        for copy in copies:
            copy.wait_recv()

    tok_x[0].start()
    start(in_y)
    start(tok_x[1:])
    start(tok_local)
    for k in kinds:
        in_local[k].start()
        in_sib[k].start()

    def normalize(s, which):
        step_rows = 64

        def step(i, carry):
            at = pl.ds(pl.multiple_of(i * step_rows, step_rows), step_rows)
            values = rows_ref[s, which, at].astype(jnp.float32)
            mean = jnp.mean(values * values, axis=-1, keepdims=True)
            rows_ref[s, which, at] = (
                values * lax.rsqrt(mean + norm_eps) * gain[...]
            ).astype(jnp.bfloat16)
            return carry

        lax.fori_loop(0, half // step_rows, step, 0)

    def project(s, which, kind):
        return jnp.dot(
            rows_ref[s, which], w_in[kind], preferred_element_type=jnp.float32
        ).astype(jnp.bfloat16)

    def stage_heads(s, which, kind):
        result = project(s, which, kind)
        for h in range(z_count):
            stage[which, kind, s, h] = result[:, h * HEAD_DIM : (h + 1) * HEAD_DIM]

    def span(owner_z, owner_x):
        return pl.ds(pl.multiple_of(owner_z * block + owner_x * half, half), half)

    for copy in tok_local:
        copy.wait()
    for s in range(seqs):
        normalize(s, 0)

    def weights_ready(k):
        in_local[k].wait()
        in_sib[k].wait_recv()
        in_y[k].wait_recv()
        in_corner[k].start()
        in_corner[k].wait_recv()

    own_copies = []
    for kind in (KEY, VALUE, QUERY):
        weights_ready(kind)

        def own_step(s, carry, kind=kind):
            stage_heads(s, 0, kind)
            heads[kind, s, span(z, x)] = stage[0, kind, s, z]
            return carry

        lax.fori_loop(0, seqs, own_step, 0)
        for by in range(z_count - 1, 0, -1):
            copy = remote(
                stage.at[0, kind, :, z_at(by)],
                heads.at[kind, :, span(z, x)],
                {"sp": z_at(by)},
            )
            copy.start()
            own_copies.append(copy)

    other_copies = []
    for s in range(seqs):
        tok_x[s].wait_recv()
        normalize(s, 1)

        def other_step(kind, carry, s=s):
            stage_heads(s, 1, kind)
            heads[kind, s, span(z, other_x)] = stage[1, kind, s, z]
            return carry

        lax.fori_loop(0, 3, other_step, 0)
        group = []
        for by in range(z_count - 1, 0, -1):
            copy = remote(
                stage.at[1, :, s, z_at(by)],
                heads.at[:, s, span(z, other_x)],
                {"sp": z_at(by)},
            )
            copy.start()
            group.append(copy)
        other_copies.append(group)

    start(out_x)
    weights_ready(POOL)
    start(out_y)
    start(out_sib)
    start(out_local)

    edge = border_out.shape[1]
    for s in range(seqs):
        for which, owner in ((0, x), (1, other_x)):
            at = pl.multiple_of(edge + owner * half, edge)
            extended[s, pl.ds(at, half)] = project(s, which, POOL).astype(jnp.float32)
        border_out[s] = extended[s, block:].astype(jnp.bfloat16)

    border = remote(border_out, border_in, {"sp": z_at(1)})

    @pl.when(z < z_count - 1)
    def send_border():
        border.start()

    @pl.when(z > 0)
    def take_border():
        border.wait_recv()
        extended[:, 0:edge] = border_in[...].astype(jnp.float32)

    @pl.when(z == 0)
    def no_border():
        extended[:, 0:edge] = jnp.zeros((seqs, edge, cols), jnp.float32)

    groups = cols // GROUP_WIDTH
    pool_copies = []
    for s in range(seqs):
        seen = (
            z * block + lax.broadcasted_iota(jnp.int32, (block, GROUP_WIDTH), 0) + 1
        ).astype(jnp.float32)
        for g in range(groups):
            at = slice(g * GROUP_WIDTH, (g + 1) * GROUP_WIDTH)
            plain = extended[s, :, at]
            total = plain
            for doubling in range(g + 1):
                total = total + pltpu.roll(total, 2**doubling, 0)
            averaged = total[edge:] / jnp.minimum(seen, float(2 ** (g + 1)))
            departure = (averaged - plain[edge:]).astype(jnp.bfloat16)
            mixed = jnp.dot(departure, mix[x * groups + g], preferred_element_type=jnp.float32)
            pool_tmp[s, :, at] = (mixed * scale[x * groups + g]).astype(jnp.bfloat16)
        lanes = pl.ds(pl.multiple_of(x * cols, cols), cols)
        pool_rows[s, :, lanes] = pool_tmp[s, pl.ds(pl.multiple_of(x * half, half), half)]
        copy = remote(
            pool_tmp.at[s, pl.ds(pl.multiple_of(other_x * half, half), half)],
            pool_rows.at[s, :, lanes],
            {"tp": other_x},
        )
        copy.start()
        pool_copies.append(copy)

    arrive(out_x)
    start(out_xy)
    start(out_xs)
    arrive(out_y)
    start(out_ys)
    arrive(own_copies)

    me = x * z_count + z
    source_count = 2 * z_count

    def attn_copy(s, dest_z, dest_x):
        return pltpu.make_async_remote_copy(
            src_ref=attn_own.at[s, pl.ds(dest_z * block + dest_x * half, half)],
            dst_ref=attn_rows.at[
                s, :, pl.ds(pl.multiple_of(me * HEAD_DIM, HEAD_DIM), HEAD_DIM)
            ],
            send_sem=attn_send.at[s, dest_z * 2 + dest_x],
            recv_sem=attn_recv.at[s, me],
            device_id={"sp": dest_z, "tp": dest_x},
            device_id_type=MESH,
        )

    def attention_block(s, index):
        low = index * block
        high = low + block
        query = heads[QUERY, s, low:high]
        gate = jnp.transpose(
            jnp.broadcast_to(gates[s, pl.ds(z, 1), low:high], (HEAD_DIM, block))
        )[:, :1]
        gate = gate * log2_e

        def scored(first, last):
            scores = lax.dot_general(
                query,
                heads[KEY, s, first:last],
                (((1,), (1,)), ((), ())),
                preferred_element_type=jnp.float32,
            )
            row = gates[s, pl.ds(z, 1), first:last] * log2_e
            return scores * (HEAD_DIM ** (-0.5) * log2_e) + (gate - row)

        def weighted(scores, top, first, last):
            lifted = jnp.exp2(scores - top)
            return jnp.sum(lifted, axis=1, keepdims=True), jnp.dot(
                lifted.astype(jnp.bfloat16),
                heads[VALUE, s, first:last],
                preferred_element_type=jnp.float32,
            )

        newest = scored(low, high)
        below = lax.broadcasted_iota(jnp.int32, newest.shape, 1) <= lax.broadcasted_iota(
            jnp.int32, newest.shape, 0
        )
        newest = jnp.where(below, newest, masked_score)
        top = jnp.max(newest, axis=1, keepdims=True)
        if low > 0:
            before = scored(0, low)
            top = jnp.maximum(top, jnp.max(before, axis=1, keepdims=True))
        denominator, total = weighted(newest, top, low, high)
        if low > 0:
            more_sum, more_total = weighted(before, top, 0, low)
            denominator = denominator + more_sum
            total = total + more_total
        attn_own[s, low:high] = (total / denominator).astype(jnp.bfloat16)

    def attention_step(s, carry):
        for index in range(z_count):
            attention_block(s, index)
            for dest_x in range(2):
                here = (z == index) & (x == dest_x)

                @pl.when(jnp.logical_not(here))
                def send(index=index, dest_x=dest_x):
                    attn_copy(s, index, dest_x).start()

                @pl.when(here)
                def keep(index=index, dest_x=dest_x):
                    first = index * block + dest_x * half
                    attn_rows[
                        s, :, pl.ds(pl.multiple_of(me * HEAD_DIM, HEAD_DIM), HEAD_DIM)
                    ] = attn_own[s, first : first + half]

        return carry

    for s in range(seqs):
        arrive(other_copies[s])
        attention_step(s, 0)

    arrive(out_xs)
    arrive(out_ys)
    arrive(out_sib)
    arrive(out_xy)
    start(out_xys)
    for copy in out_local:
        copy.wait()
    arrive(out_xys)

    def out_copy(s):
        return pltpu.make_async_copy(out_stage.at[s], out.at[s], local_sem.at[s])

    tile = min(512, width)

    def output_step(s, carry):
        for by in range(1, source_count):
            source = lax.rem(me + by, source_count)
            pltpu.make_async_copy(
                attn_rows.at[s, :, 0:HEAD_DIM],
                attn_rows.at[s, :, 0:HEAD_DIM],
                attn_recv.at[s, source],
            ).wait()

        def tile_step(n, inner):
            lanes = pl.ds(pl.multiple_of(n * tile, tile), tile)
            result = jnp.dot(
                pool_rows[s], w_out[0, :, lanes], preferred_element_type=jnp.float32
            ) + jnp.dot(attn_rows[s], w_out[1, :, lanes], preferred_element_type=jnp.float32)
            out_stage[s, :, lanes] = result.astype(jnp.bfloat16)
            return inner

        lax.fori_loop(0, width // tile, tile_step, 0)
        out_copy(s).start()
        return carry

    arrive(pool_copies)
    lax.fori_loop(0, seqs, output_step, 0)

    for group in (
        tok_x, in_y, in_sib, in_corner, out_x, out_y, out_sib, out_xy, out_xs, out_ys, out_xys,
        own_copies, *other_copies, pool_copies,
    ):
        for copy in group:
            copy.wait_send()

    @pl.when(z < z_count - 1)
    def border_sent():
        border.wait_send()

    for s in range(seqs):
        for dest_z in range(z_count):
            for dest_x in range(2):

                @pl.when(jnp.logical_not((z == dest_z) & (x == dest_x)))
                def sent(s=s, dest_z=dest_z, dest_x=dest_x):
                    attn_copy(s, dest_z, dest_x).wait_send()

        out_copy(s).wait()


def fast_device(
    tokens,
    norm_gain,
    w_pool_in,
    pool_mix,
    pool_scale,
    w_query,
    w_key,
    w_value,
    gate_cache,
    w_out_pool,
    w_out_attn,
):
    seqs, half, width = tokens.shape
    block = 2 * half
    cols = w_key.shape[1]
    z_count = lax.axis_size("sp")
    length = block * z_count
    edge = 16
    bf16 = jnp.bfloat16
    anywhere = pl.BlockSpec(memory_space=pl.ANY)
    inside = pl.BlockSpec(memory_space=pltpu.VMEM)
    dma = pltpu.SemaphoreType.DMA
    return pl.pallas_call(
        layer_kernel,
        in_specs=[
            anywhere,
            inside,
            anywhere,
            inside,
            inside,
            anywhere,
            anywhere,
            anywhere,
            inside,
            anywhere,
            anywhere,
        ],
        out_specs=anywhere,
        out_shape=jax.ShapeDtypeStruct(tokens.shape, bf16),
        scratch_shapes=[
            pltpu.VMEM((4, width, cols), bf16),
            pltpu.VMEM((2, 2 * cols, width), bf16),
            pltpu.VMEM((seqs, 2, half, width), bf16),
            pltpu.VMEM((2, 3, seqs, z_count, half, HEAD_DIM), bf16),
            pltpu.VMEM((3, seqs, length, HEAD_DIM), bf16),
            pltpu.VMEM((seqs, edge + block, cols), jnp.float32),
            pltpu.VMEM((seqs, edge, cols), bf16),
            pltpu.VMEM((seqs, edge, cols), bf16),
            pltpu.VMEM((seqs, block, cols), bf16),
            pltpu.VMEM((seqs, half, 2 * cols), bf16),
            pltpu.VMEM((seqs, length, HEAD_DIM), bf16),
            pltpu.VMEM((seqs, half, 2 * cols), bf16),
            pltpu.VMEM((seqs, half, width), bf16),
            dma((16,)),
            dma((96,)),
            dma((96,)),
            dma((seqs, 2 * z_count)),
            dma((seqs, 2 * z_count)),
        ],
        compiler_params=pltpu.CompilerParams(
            collective_id=0,
            has_side_effects=True,
            vmem_limit_bytes=60 * 1024 * 1024,
        ),
    )(
        tokens,
        norm_gain.reshape(1, width),
        w_pool_in,
        pool_mix,
        pool_scale.reshape(-1, 1, GROUP_WIDTH),
        w_query,
        w_key,
        w_value,
        gate_cache,
        w_out_pool,
        w_out_attn,
    )


def on_device(*args):
    cols = args[5].shape[1]
    half = args[0].shape[1]
    sp_count = lax.axis_size("sp")
    suited = (
        lax.axis_size("tp") == 2
        and lax.axis_size("fs") == 4
        and cols == sp_count * HEAD_DIM
        and args[2].shape[1] == cols == 4 * GROUP_WIDTH
        and half % 128 == 0
        and args[0].shape[2] == 4 * cols
        and half * 2 * sp_count <= 2048
        and args[0].shape[0] <= 2
    )
    if suited:
        return fast_device(*args)
    return general_device(*args)


def solution(mesh):
    placed = (
        P("fs", ("sp", "tp"), None),
        P(),
        P("fs", "tp"),
        P(),
        P(),
        P("fs", "tp"),
        P("fs", "tp"),
        P("fs", "tp"),
        P("fs", "tp", None),
        P("tp", "fs"),
        P("tp", "fs"),
    )
    return jax.shard_map(
        on_device,
        mesh=mesh,
        in_specs=placed,
        out_specs=P("fs", ("sp", "tp"), None),
        check_vma=False,
    )
```

profile of v0, /device:TPU:16, one launch (start us, length us, event | category | flops | bytes accessed | tf_op | source)
XLA Modules:
  0.0 135.1 jit_solution(12534939745747588357)
XLA Ops:
  0.0 132.0 %shard_map.109 = bf16[2,256,2048]{2,1,0:T(8,128)(2,1)} custom-call(bf16[2,256,2048]{2,1,0:T(8,128)(2,1)} %tokens.1, f32[1,2048]{1,0:T(1,128)} %bitcast.2, bf16[512,512]{1,0:T(8,128)(2,1)} %w_pool.1, bf16[8,128,128]{2,1,0:T(8,128)(2,1)} %mix.1, f32[8,1,128]{2,1,0:T(1,128)} %bitcast.3, bf16[512,512]{1,0:T(8,128)(2,1)} %w_query.1, bf16[512,512]{1,0:T(8,128)(2,1)} %w_key.1, ...), custom_call_target="tpu_custom_call" | custom-call | tf_op jit(solution)/shard_map/pallas_call | solution.py:647
  132.0 3.2 %copy.13 = bf16[2,256,2048]{2,1,0:T(8,128)(2,1)} copy(bf16[2,256,2048]{2,1,0:T(8,128)(2,1)} %shard_map.109) | data formatting | bytes 4194304
where the time goes:
time: 135 us
  Pallas kernels  132 us (98%)
  local copies, waits for them, and re-layouts  3.16 us (2%)
    pallas_call x1, Pallas kernels, fast_device(): pl.pallas_call(layer_kernel, in_specs=[anywhere, inside, anywhere, inside...  132 us
    unnamed x1, local copies, waits for them, and re-layouts  3.16 us

commit v1 on v0

--- a/solution.py
+++ b/solution.py
@@ -230,11 +230,9 @@
     w_in,
     w_out,
     rows_ref,
-    stage,
     heads,
     extended,
-    border_out,
-    border_in,
+    border,
     pool_tmp,
     pool_rows,
     attn_own,
@@ -243,6 +241,8 @@
     local_sem,
     send_sem,
     recv_sem,
+    z_send,
+    z_recv,
     attn_send,
     attn_recv,
 ):
@@ -255,7 +255,8 @@
     other_x = 1 - x
     sibling = f + 1 - 2 * lax.rem(f, 2)
     across = lax.rem(f + 2, 4)
-    z_count = stage.shape[3]
+    z_count = heads.shape[2]
+    edge = border.shape[1]
 
     def z_at(by):
         return lax.rem(z + by, z_count)
@@ -287,8 +288,10 @@
     def local(source, target):
         return pltpu.make_async_copy(source, target, local_sem.at[next(local_numbers)])
 
-    def in_slot(kind, owner):
-        return w_in.at[kind, pl.ds(pl.multiple_of(owner * depth, depth), depth)]
+    def in_slot(piece, owner):
+        kind, low, high = piece
+        at = pl.multiple_of(owner * depth, depth)
+        return w_in.at[kind, pl.ds(at, depth), low:high]
 
     def out_slot(kind, owner_x, owner_f):
         return w_out.at[
@@ -299,12 +302,20 @@
 
     w_own = (w_key, w_value, w_query, w_pool)
     out_own = (w_out_pool, w_out_attn)
-    kinds = range(4)
+    pair = 2 * HEAD_DIM
+    pieces = [
+        (kind, low, low + pair) for kind in (KEY, VALUE, QUERY) for low in range(0, cols, pair)
+    ]
+    pieces.append((POOL, 0, cols))
+
+    def own_piece(piece):
+        kind, low, high = piece
+        return w_own[kind].at[:, low:high]
 
     tok_x = [remote(tokens.at[s], rows_ref.at[s, 1], {"tp": other_x}) for s in range(seqs)]
-    in_y = [remote(w_own[k], in_slot(k, f), {"fs": across}) for k in kinds]
-    in_sib = [remote(w_own[k], in_slot(k, f), {"fs": sibling}) for k in kinds]
-    in_corner = [remote(in_slot(k, across), in_slot(k, across), {"fs": sibling}) for k in kinds]
+    in_y = [remote(own_piece(p), in_slot(p, f), {"fs": across}) for p in pieces]
+    in_sib = [remote(own_piece(p), in_slot(p, f), {"fs": sibling}) for p in pieces]
+    in_corner = [remote(in_slot(p, across), in_slot(p, across), {"fs": sibling}) for p in pieces]
     out_x = [remote(out_own[k], out_slot(k, x, f), {"tp": other_x}) for k in range(2)]
     out_y = [remote(out_own[k], out_slot(k, x, f), {"fs": across}) for k in range(2)]
     out_sib = [remote(out_own[k], out_slot(k, x, f), {"fs": sibling}) for k in range(2)]
@@ -320,7 +331,7 @@
     out_ys = forwarded(x, across, {"fs": sibling})
     out_xys = forwarded(other_x, across, {"fs": sibling})
     tok_local = [local(tokens.at[s], rows_ref.at[s, 0]) for s in range(seqs)]
-    in_local = [local(w_own[k], in_slot(k, f)) for k in kinds]
+    in_local = [local(own_piece(p), in_slot(p, f)) for p in pieces]
     out_local = [local(out_own[k], out_slot(k, x, f)) for k in range(2)]
 
     def start(copies):
@@ -330,38 +341,65 @@
     def arrive(copies):
         for copy in copies:
             copy.wait_recv()
+
+    border_number = next(numbers)
+    next(numbers)
+
+    def border_copy(dest_x):
+        return pltpu.make_async_remote_copy(
+            src_ref=tokens.at[:, half - edge :],
+            dst_ref=border,
+            send_sem=send_sem.at[border_number + dest_x],
+            recv_sem=recv_sem.at[border_number],
+            device_id={"sp": z_at(1), "tp": dest_x},
+            device_id_type=MESH,
+        )
+
+    sends_border = (z < z_count - 1) & (x == 1)
 
     tok_x[0].start()
     start(in_y)
     start(tok_x[1:])
     start(tok_local)
-    for k in kinds:
-        in_local[k].start()
-        in_sib[k].start()
+    for copy, copy_sib in zip(in_local, in_sib):
+        copy.start()
+        copy_sib.start()
+
+    @pl.when(sends_border)
+    def send_border():
+        for dest_x in range(2):
+            border_copy(dest_x).start()
+
+    start(out_x)
+    start(out_y)
+    start(out_sib)
+    start(out_local)
+
+    def normalized(rows):
+        values = rows.astype(jnp.float32)
+        mean = jnp.mean(values * values, axis=-1, keepdims=True)
+        return (values * lax.rsqrt(mean + norm_eps) * gain[...]).astype(jnp.bfloat16)
 
     def normalize(s, which):
         step_rows = 64
 
         def step(i, carry):
             at = pl.ds(pl.multiple_of(i * step_rows, step_rows), step_rows)
-            values = rows_ref[s, which, at].astype(jnp.float32)
-            mean = jnp.mean(values * values, axis=-1, keepdims=True)
-            rows_ref[s, which, at] = (
-                values * lax.rsqrt(mean + norm_eps) * gain[...]
-            ).astype(jnp.bfloat16)
+            rows_ref[s, which, at] = normalized(rows_ref[s, which, at])
             return carry
 
         lax.fori_loop(0, half // step_rows, step, 0)
 
-    def project(s, which, kind):
+    def project(values, kind, low=0, high=cols):
         return jnp.dot(
-            rows_ref[s, which], w_in[kind], preferred_element_type=jnp.float32
+            values, w_in[kind, :, low:high], preferred_element_type=jnp.float32
         ).astype(jnp.bfloat16)
 
-    def stage_heads(s, which, kind):
-        result = project(s, which, kind)
-        for h in range(z_count):
-            stage[which, kind, s, h] = result[:, h * HEAD_DIM : (h + 1) * HEAD_DIM]
+    def project_heads(s, which, kind, low, high):
+        result = project(rows_ref[s, which], kind, low, high)
+        at = span(z, x if which == 0 else other_x)
+        for h in range(low // HEAD_DIM, high // HEAD_DIM):
+            heads[kind, s, h, at] = result[:, h * HEAD_DIM - low : (h + 1) * HEAD_DIM - low]
 
     def span(owner_z, owner_x):
         return pl.ds(pl.multiple_of(owner_z * block + owner_x * half, half), half)
@@ -378,70 +416,105 @@
         in_corner[k].start()
         in_corner[k].wait_recv()
 
-    own_copies = []
+    def z_copy(group, kinds, dest, which, which_seqs, first, last):
+        at = span(z, x if which == 0 else other_x)
+        view = heads.at[kinds, which_seqs, first:last, at]
+        return pltpu.make_async_remote_copy(
+            src_ref=view,
+            dst_ref=view,
+            send_sem=z_send.at[group, dest if last - first == 1 else z_count],
+            recv_sem=z_recv.at[group, z if last - first == 1 else z_count],
+            device_id={"sp": dest},
+            device_id_type=MESH,
+        )
+
+    def queries_go(dest):
+        return z >= 1 if dest == 0 else z >= z_count // 2
+
+    everything = pl.ds(0, seqs)
+    groups_z = []
     for kind in (KEY, VALUE, QUERY):
-        weights_ready(kind)
-
-        def own_step(s, carry, kind=kind):
-            stage_heads(s, 0, kind)
-            heads[kind, s, span(z, x)] = stage[0, kind, s, z]
+        groups_z.append((pl.ds(kind, 1), 0, everything))
+    for s in range(seqs):
+        groups_z.append((pl.ds(KEY, 2), 1, pl.ds(s, 1)))
+        groups_z.append((pl.ds(QUERY, 1), 1, pl.ds(s, 1)))
+    asks = [g == QUERY or (g > QUERY and (g - QUERY) % 2 == 0) for g in range(len(groups_z))]
+    middle = z_count // 2
+
+    def each_send(group, dests, act):
+        kinds, which, which_seqs = groups_z[group]
+        for dest in dests:
+            going = z != dest
+            if asks[group]:
+                going = going & queries_go(dest)
+
+            @pl.when(going)
+            def to(dest=dest):
+                act(z_copy(group, kinds, dest, which, which_seqs, dest, dest + 1))
+
+        if not asks[group] and dests[0] >= middle:
+
+            @pl.when(z == 0)
+            def to_next():
+                act(z_copy(group, kinds, 1, which, which_seqs, middle, z_count))
+
+    def each_recv(group):
+        kinds, which, which_seqs = groups_z[group]
+        for source in range(z_count):
+            coming = z != source
+            if asks[group]:
+                coming = coming & ((z == 0) if source == 1 else (source >= middle))
+
+            @pl.when(coming)
+            def came(source=source):
+                view = heads.at[kinds, which_seqs, 0:1, pl.ds(0, half)]
+                pltpu.make_async_copy(view, view, z_recv.at[group, source]).wait()
+
+        if not asks[group]:
+
+            @pl.when(z == 1)
+            def came_next():
+                view = heads.at[kinds, which_seqs, middle:z_count, pl.ds(0, half)]
+                pltpu.make_async_copy(view, view, z_recv.at[group, z_count]).wait()
+
+    left_dests = tuple(range(middle))
+    right_dests = tuple(range(z_count - 1, middle - 1, -1))
+
+    for number, (kind, low, high) in enumerate(pieces[:-1]):
+        weights_ready(number)
+
+        def own_step(s, carry, kind=kind, low=low, high=high):
+            project_heads(s, 0, kind, low, high)
             return carry
 
         lax.fori_loop(0, seqs, own_step, 0)
-        for by in range(z_count - 1, 0, -1):
-            copy = remote(
-                stage.at[0, kind, :, z_at(by)],
-                heads.at[kind, :, span(z, x)],
-                {"sp": z_at(by)},
-            )
-            copy.start()
-            own_copies.append(copy)
-
-    other_copies = []
+        each_send(kind, left_dests if low == 0 else right_dests, lambda copy: copy.start())
+
     for s in range(seqs):
         tok_x[s].wait_recv()
         normalize(s, 1)
-
-        def other_step(kind, carry, s=s):
-            stage_heads(s, 1, kind)
-            heads[kind, s, span(z, other_x)] = stage[1, kind, s, z]
-            return carry
-
-        lax.fori_loop(0, 3, other_step, 0)
-        group = []
-        for by in range(z_count - 1, 0, -1):
-            copy = remote(
-                stage.at[1, :, s, z_at(by)],
-                heads.at[:, s, span(z, other_x)],
-                {"sp": z_at(by)},
-            )
-            copy.start()
-            group.append(copy)
-        other_copies.append(group)
-
-    start(out_x)
-    weights_ready(POOL)
-    start(out_y)
-    start(out_sib)
-    start(out_local)
-
-    edge = border_out.shape[1]
+        for group, kinds in ((3 + 2 * s, (KEY, VALUE)), (4 + 2 * s, (QUERY,))):
+
+            def other_step(kind, carry, s=s):
+                project_heads(s, 1, kind, 0, cols)
+                return carry
+
+            lax.fori_loop(kinds[0], kinds[-1] + 1, other_step, 0)
+            each_send(group, left_dests, lambda copy: copy.start())
+            each_send(group, right_dests, lambda copy: copy.start())
+
+    weights_ready(len(pieces) - 1)
     for s in range(seqs):
         for which, owner in ((0, x), (1, other_x)):
             at = pl.multiple_of(edge + owner * half, edge)
-            extended[s, pl.ds(at, half)] = project(s, which, POOL).astype(jnp.float32)
-        border_out[s] = extended[s, block:].astype(jnp.bfloat16)
-
-    border = remote(border_out, border_in, {"sp": z_at(1)})
-
-    @pl.when(z < z_count - 1)
-    def send_border():
-        border.start()
+            extended[s, pl.ds(at, half)] = project(rows_ref[s, which], POOL).astype(jnp.float32)
 
     @pl.when(z > 0)
     def take_border():
-        border.wait_recv()
-        extended[:, 0:edge] = border_in[...].astype(jnp.float32)
+        border_copy(0).wait_recv()
+        for s in range(seqs):
+            values = normalized(border[s])
+            extended[s, 0:edge] = project(values, POOL).astype(jnp.float32)
 
     @pl.when(z == 0)
     def no_border():
@@ -478,47 +551,47 @@
     start(out_xs)
     arrive(out_y)
     start(out_ys)
-    arrive(own_copies)
-
-    me = x * z_count + z
-    source_count = 2 * z_count
-
-    def attn_copy(s, dest_z, dest_x):
+
+
+    def head_lanes(owner_x, head):
+        at = pl.multiple_of((owner_x * z_count + head) * HEAD_DIM, HEAD_DIM)
+        return pl.ds(at, HEAD_DIM)
+
+    def attn_copy(s, index, head, dest_x):
+        first = index * block + dest_x * half
         return pltpu.make_async_remote_copy(
-            src_ref=attn_own.at[s, pl.ds(dest_z * block + dest_x * half, half)],
-            dst_ref=attn_rows.at[
-                s, :, pl.ds(pl.multiple_of(me * HEAD_DIM, HEAD_DIM), HEAD_DIM)
-            ],
-            send_sem=attn_send.at[s, dest_z * 2 + dest_x],
-            recv_sem=attn_recv.at[s, me],
-            device_id={"sp": dest_z, "tp": dest_x},
+            src_ref=attn_own.at[s, head, first : first + half],
+            dst_ref=attn_rows.at[s, :, head_lanes(x, head)],
+            send_sem=attn_send.at[s, index, head, dest_x],
+            recv_sem=attn_recv.at[s, x * z_count + head],
+            device_id={"sp": index, "tp": dest_x},
             device_id_type=MESH,
         )
 
-    def attention_block(s, index):
+    def attention_block(s, index, head):
         low = index * block
         high = low + block
-        query = heads[QUERY, s, low:high]
+        query = heads[QUERY, s, head, low:high]
         gate = jnp.transpose(
-            jnp.broadcast_to(gates[s, pl.ds(z, 1), low:high], (HEAD_DIM, block))
+            jnp.broadcast_to(gates[s, pl.ds(head, 1), low:high], (HEAD_DIM, block))
         )[:, :1]
         gate = gate * log2_e
 
         def scored(first, last):
             scores = lax.dot_general(
                 query,
-                heads[KEY, s, first:last],
+                heads[KEY, s, head, first:last],
                 (((1,), (1,)), ((), ())),
                 preferred_element_type=jnp.float32,
             )
-            row = gates[s, pl.ds(z, 1), first:last] * log2_e
+            row = gates[s, pl.ds(head, 1), first:last] * log2_e
             return scores * (HEAD_DIM ** (-0.5) * log2_e) + (gate - row)
 
         def weighted(scores, top, first, last):
             lifted = jnp.exp2(scores - top)
             return jnp.sum(lifted, axis=1, keepdims=True), jnp.dot(
                 lifted.astype(jnp.bfloat16),
-                heads[VALUE, s, first:last],
+                heads[VALUE, s, head, first:last],
                 preferred_element_type=jnp.float32,
             )
 
@@ -536,30 +609,52 @@
             more_sum, more_total = weighted(before, top, 0, low)
             denominator = denominator + more_sum
             total = total + more_total
-        attn_own[s, low:high] = (total / denominator).astype(jnp.bfloat16)
-
-    def attention_step(s, carry):
-        for index in range(z_count):
-            attention_block(s, index)
+        attn_own[s, head, low:high] = (total / denominator).astype(jnp.bfloat16)
+
+    def attention_rows(s, index, first_head, last_head):
+        def head_step(head, carry):
+            attention_block(s, index, head)
             for dest_x in range(2):
                 here = (z == index) & (x == dest_x)
 
                 @pl.when(jnp.logical_not(here))
-                def send(index=index, dest_x=dest_x):
-                    attn_copy(s, index, dest_x).start()
+                def send(dest_x=dest_x):
+                    attn_copy(s, index, head, dest_x).start()
 
                 @pl.when(here)
-                def keep(index=index, dest_x=dest_x):
+                def keep(dest_x=dest_x):
                     first = index * block + dest_x * half
-                    attn_rows[
-                        s, :, pl.ds(pl.multiple_of(me * HEAD_DIM, HEAD_DIM), HEAD_DIM)
-                    ] = attn_own[s, first : first + half]
-
-        return carry
+                    attn_rows[s, :, head_lanes(x, head)] = attn_own[
+                        s, head, first : first + half
+                    ]
+
+            return carry
+
+        lax.fori_loop(first_head, last_head, head_step, 0)
+
+    def heads_of(index):
+        if index == 0:
+            return 0, z_count
+        if index == 1:
+            return z, 1 + (z_count - 1) * z
+        return z, z + 1
 
     for s in range(seqs):
-        arrive(other_copies[s])
-        attention_step(s, 0)
+
+        @pl.when(z == 0)
+        def first_rows(s=s):
+            attention_rows(s, 0, *heads_of(0))
+
+    for s in range(seqs):
+        for group in ((KEY, VALUE, QUERY) if s == 0 else ()) + (3 + 2 * s, 4 + 2 * s):
+            each_recv(group)
+
+        @pl.when(z < 2)
+        def second_rows(s=s):
+            attention_rows(s, 1, *heads_of(1))
+
+        for index in range(2, z_count):
+            attention_rows(s, index, *heads_of(index))
 
     arrive(out_xs)
     arrive(out_ys)
@@ -576,13 +671,15 @@
     tile = min(512, width)
 
     def output_step(s, carry):
-        for by in range(1, source_count):
-            source = lax.rem(me + by, source_count)
-            pltpu.make_async_copy(
-                attn_rows.at[s, :, 0:HEAD_DIM],
-                attn_rows.at[s, :, 0:HEAD_DIM],
-                attn_recv.at[s, source],
-            ).wait()
+        for source_x in range(2):
+            for head in range(z_count):
+                made_here = (z == 0) | (z == head) | ((z == 1) & (head > 0))
+
+                @pl.when(jnp.logical_not((x == source_x) & made_here))
+                def came(source_x=source_x, head=head):
+                    view = attn_rows.at[s, :, 0:HEAD_DIM]
+                    number = source_x * z_count + head
+                    pltpu.make_async_copy(view, view, attn_recv.at[s, number]).wait()
 
         def tile_step(n, inner):
             lanes = pl.ds(pl.multiple_of(n * tile, tile), tile)
@@ -601,23 +698,37 @@
 
     for group in (
         tok_x, in_y, in_sib, in_corner, out_x, out_y, out_sib, out_xy, out_xs, out_ys, out_xys,
-        own_copies, *other_copies, pool_copies,
+        pool_copies,
     ):
         for copy in group:
             copy.wait_send()
 
-    @pl.when(z < z_count - 1)
+    @pl.when(sends_border)
     def border_sent():
-        border.wait_send()
+        for dest_x in range(2):
+            border_copy(dest_x).wait_send()
+
+    for group in range(len(groups_z)):
+        each_send(group, left_dests, lambda copy: copy.wait_send())
+        each_send(group, right_dests, lambda copy: copy.wait_send())
+
+    def attention_sent(s, index):
+        def head_step(head, carry):
+            for dest_x in range(2):
+
+                @pl.when(jnp.logical_not((z == index) & (x == dest_x)))
+                def sent(dest_x=dest_x):
+                    attn_copy(s, index, head, dest_x).wait_send()
+
+            return carry
+
+        lax.fori_loop(*heads_of(index), head_step, 0)
 
     for s in range(seqs):
-        for dest_z in range(z_count):
-            for dest_x in range(2):
-
-                @pl.when(jnp.logical_not((z == dest_z) & (x == dest_x)))
-                def sent(s=s, dest_z=dest_z, dest_x=dest_x):
-                    attn_copy(s, dest_z, dest_x).wait_send()
-
+        pl.when(z == 0)(lambda s=s: attention_sent(s, 0))
+        pl.when(z < 2)(lambda s=s: attention_sent(s, 1))
+        for index in range(2, z_count):
+            attention_sent(s, index)
         out_copy(s).wait()
 
 
@@ -665,20 +776,20 @@
             pltpu.VMEM((4, width, cols), bf16),
             pltpu.VMEM((2, 2 * cols, width), bf16),
             pltpu.VMEM((seqs, 2, half, width), bf16),
-            pltpu.VMEM((2, 3, seqs, z_count, half, HEAD_DIM), bf16),
-            pltpu.VMEM((3, seqs, length, HEAD_DIM), bf16),
+            pltpu.VMEM((3, seqs, z_count, length, HEAD_DIM), bf16),
             pltpu.VMEM((seqs, edge + block, cols), jnp.float32),
-            pltpu.VMEM((seqs, edge, cols), bf16),
-            pltpu.VMEM((seqs, edge, cols), bf16),
+            pltpu.VMEM((seqs, edge, width), bf16),
             pltpu.VMEM((seqs, block, cols), bf16),
             pltpu.VMEM((seqs, half, 2 * cols), bf16),
-            pltpu.VMEM((seqs, length, HEAD_DIM), bf16),
+            pltpu.VMEM((seqs, z_count, length, HEAD_DIM), bf16),
             pltpu.VMEM((seqs, half, 2 * cols), bf16),
             pltpu.VMEM((seqs, half, width), bf16),
             dma((16,)),
-            dma((96,)),
-            dma((96,)),
-            dma((seqs, 2 * z_count)),
+            dma((64,)),
+            dma((64,)),
+            dma((3 + 2 * seqs, z_count + 1)),
+            dma((3 + 2 * seqs, z_count + 1)),
+            dma((seqs, z_count, z_count, 2)),
             dma((seqs, 2 * z_count)),
         ],
         compiler_params=pltpu.CompilerParams(
@@ -713,6 +824,7 @@
         and half % 128 == 0
         and args[0].shape[2] == 4 * cols
         and half * 2 * sp_count <= 2048
+        and sp_count == 4
         and args[0].shape[0] <= 2
     )
     if suited:

time: 135 us -> 117 us (0.87)
  the two profiles are of different devices: /device:TPU:16 before, /device:TPU:27 now
where the time goes in v1:
time: 117 us; the launch traced here: 116 us
  Pallas kernels  113 us (97%)
  local copies, waits for them, and re-layouts  3.16 us (3%)
    pallas_call x1, Pallas kernels, fast_device(): pl.pallas_call(layer_kernel, in_specs=[anywhere, inside, anywhere, inside...  113 us
    unnamed x1, local copies, waits for them, and re-layouts  3.16 us

profile of v1, /device:TPU:27, one launch (start us, length us, event | category | flops | bytes accessed | tf_op | source)
XLA Modules:
  0.0 116.0 jit_solution(7729094042984852605)
XLA Ops:
  0.0 112.8 %shard_map.109 = bf16[2,256,2048]{2,1,0:T(8,128)(2,1)} custom-call(bf16[2,256,2048]{2,1,0:T(8,128)(2,1)} %tokens.1, f32[1,2048]{1,0:T(1,128)} %bitcast.2, bf16[512,512]{1,0:T(8,128)(2,1)} %w_pool.1, bf16[8,128,128]{2,1,0:T(8,128)(2,1)} %mix.1, f32[8,1,128]{2,1,0:T(1,128)} %bitcast.3, bf16[512,512]{1,0:T(8,128)(2,1)} %w_query.1, bf16[512,512]{1,0:T(8,128)(2,1)} %w_key.1, ...), custom_call_target="tpu_custom_call" | custom-call | tf_op jit(solution)/shard_map/pallas_call | solution.py:758
  112.8 3.2 %copy.13 = bf16[2,256,2048]{2,1,0:T(8,128)(2,1)} copy(bf16[2,256,2048]{2,1,0:T(8,128)(2,1)} %shard_map.109) | data formatting | bytes 4194304

commit v2 on v1

--- a/solution.py
+++ b/solution.py
@@ -216,17 +216,21 @@
 
 def layer_kernel(
     tokens,
-    gain,
+    gain_in,
     w_pool,
-    mix,
-    scale,
+    mix_in,
+    scale_in,
     w_query,
     w_key,
     w_value,
-    gates,
+    gates_in,
     w_out_pool,
     w_out_attn,
     out,
+    gain,
+    mix,
+    scale,
+    gates,
     w_in,
     w_out,
     rows_ref,
@@ -237,7 +241,7 @@
     pool_rows,
     attn_own,
     attn_rows,
-    out_stage,
+    pooled,
     local_sem,
     send_sem,
     recv_sem,
@@ -245,6 +249,8 @@
     z_recv,
     attn_send,
     attn_recv,
+    border_sem,
+    pass_send,
 ):
     z = lax.axis_index("sp")
     f = lax.axis_index("fs")
@@ -293,6 +299,11 @@
         at = pl.multiple_of(owner * depth, depth)
         return w_in.at[kind, pl.ds(at, depth), low:high]
 
+    def in_part(piece, owner, part):
+        kind, low, high = piece
+        at = pl.multiple_of(owner * depth + part * (depth // 2), depth // 2)
+        return w_in.at[kind, pl.ds(at, depth // 2), low:high]
+
     def out_slot(kind, owner_x, owner_f):
         return w_out.at[
             kind,
@@ -313,9 +324,29 @@
         return w_own[kind].at[:, low:high]
 
     tok_x = [remote(tokens.at[s], rows_ref.at[s, 1], {"tp": other_x}) for s in range(seqs)]
-    in_y = [remote(own_piece(p), in_slot(p, f), {"fs": across}) for p in pieces]
+    parity = lax.rem(z, 2)
+    partner = z + 1 - 2 * parity
+    shared = [p for p in pieces if p[0] == KEY]
+    in_y = []
+    in_z = []
+    in_corner_other = []
+    for p in pieces:
+        if p in shared:
+            kind, low, high = p
+            at = pl.multiple_of(parity * (depth // 2), depth // 2)
+            source = w_own[kind].at[pl.ds(at, depth // 2), low:high]
+            in_y.append(remote(source, in_part(p, f, parity), {"fs": across}))
+            view = in_part(p, across, parity)
+            in_z.append(remote(view, view, {"sp": partner}))
+            view = in_part(p, across, 1 - parity)
+            in_corner_other.append(remote(view, view, {"fs": sibling}))
+        else:
+            in_y.append(remote(own_piece(p), in_slot(p, f), {"fs": across}))
     in_sib = [remote(own_piece(p), in_slot(p, f), {"fs": sibling}) for p in pieces]
-    in_corner = [remote(in_slot(p, across), in_slot(p, across), {"fs": sibling}) for p in pieces]
+    in_corner = []
+    for p in pieces:
+        view = in_part(p, across, parity) if p in shared else in_slot(p, across)
+        in_corner.append(remote(view, view, {"fs": sibling}))
     out_x = [remote(out_own[k], out_slot(k, x, f), {"tp": other_x}) for k in range(2)]
     out_y = [remote(out_own[k], out_slot(k, x, f), {"fs": across}) for k in range(2)]
     out_sib = [remote(out_own[k], out_slot(k, x, f), {"fs": sibling}) for k in range(2)]
@@ -330,6 +361,12 @@
     out_xs = forwarded(other_x, f, {"fs": sibling})
     out_ys = forwarded(x, across, {"fs": sibling})
     out_xys = forwarded(other_x, across, {"fs": sibling})
+    small_local = [
+        local(gain_in, gain),
+        local(mix_in, mix),
+        local(scale_in, scale),
+        local(gates_in, gates),
+    ]
     tok_local = [local(tokens.at[s], rows_ref.at[s, 0]) for s in range(seqs)]
     in_local = [local(own_piece(p), in_slot(p, f)) for p in pieces]
     out_local = [local(out_own[k], out_slot(k, x, f)) for k in range(2)]
@@ -342,37 +379,33 @@
         for copy in copies:
             copy.wait_recv()
 
-    border_number = next(numbers)
-    next(numbers)
-
-    def border_copy(dest_x):
+    def border_copy(s, which):
         return pltpu.make_async_remote_copy(
-            src_ref=tokens.at[:, half - edge :],
-            dst_ref=border,
-            send_sem=send_sem.at[border_number + dest_x],
-            recv_sem=recv_sem.at[border_number],
-            device_id={"sp": z_at(1), "tp": dest_x},
+            src_ref=rows_ref.at[s, which, half - edge :],
+            dst_ref=border.at[s],
+            send_sem=border_sem.at[0, s],
+            recv_sem=border_sem.at[1, s],
+            device_id={"sp": z_at(1)},
             device_id_type=MESH,
         )
 
-    sends_border = (z < z_count - 1) & (x == 1)
+    def each_border(s, act):
+        for which, owner in ((0, 1), (1, 0)):
+
+            @pl.when((z < z_count - 1) & (x == owner))
+            def to_next(which=which):
+                act(border_copy(s, which))
 
     tok_x[0].start()
     start(in_y)
     start(tok_x[1:])
     start(tok_local)
-    for copy, copy_sib in zip(in_local, in_sib):
-        copy.start()
-        copy_sib.start()
-
-    @pl.when(sends_border)
-    def send_border():
-        for dest_x in range(2):
-            border_copy(dest_x).start()
+    start(small_local)
+    start(in_local)
+    start(in_sib[:2])
 
     start(out_x)
     start(out_y)
-    start(out_sib)
     start(out_local)
 
     def normalized(rows):
@@ -404,16 +437,24 @@
     def span(owner_z, owner_x):
         return pl.ds(pl.multiple_of(owner_z * block + owner_x * half, half), half)
 
-    for copy in tok_local:
+    for copy in tok_local + small_local:
         copy.wait()
     for s in range(seqs):
         normalize(s, 0)
 
+    def weights_landed(k):
+        in_y[k].wait_recv()
+        if k < len(shared):
+            in_z[k].start()
+        in_corner[k].start()
+
     def weights_ready(k):
         in_local[k].wait()
         in_sib[k].wait_recv()
-        in_y[k].wait_recv()
-        in_corner[k].start()
+        if k < len(shared):
+            in_z[k].wait_recv()
+            in_corner_other[k].start()
+            in_corner_other[k].wait_recv()
         in_corner[k].wait_recv()
 
     def z_copy(group, kinds, dest, which, which_seqs, first, last):
@@ -447,6 +488,8 @@
             going = z != dest
             if asks[group]:
                 going = going & queries_go(dest)
+            elif dest >= middle:
+                going = going & (z > 0)
 
             @pl.when(going)
             def to(dest=dest):
@@ -458,9 +501,9 @@
             def to_next():
                 act(z_copy(group, kinds, 1, which, which_seqs, middle, z_count))
 
-    def each_recv(group):
+    def each_recv(group, sources):
         kinds, which, which_seqs = groups_z[group]
-        for source in range(z_count):
+        for source in sources:
             coming = z != source
             if asks[group]:
                 coming = coming & ((z == 0) if source == 1 else (source >= middle))
@@ -470,17 +513,40 @@
                 view = heads.at[kinds, which_seqs, 0:1, pl.ds(0, half)]
                 pltpu.make_async_copy(view, view, z_recv.at[group, source]).wait()
 
-        if not asks[group]:
-
-            @pl.when(z == 1)
-            def came_next():
-                view = heads.at[kinds, which_seqs, middle:z_count, pl.ds(0, half)]
-                pltpu.make_async_copy(view, view, z_recv.at[group, z_count]).wait()
+    def pass_copy(group, dest):
+        kinds, which, which_seqs = groups_z[group]
+        at = span(0, x if which == 0 else other_x)
+        view = heads.at[kinds, which_seqs, dest : dest + 1, at]
+        return pltpu.make_async_remote_copy(
+            src_ref=view,
+            dst_ref=view,
+            send_sem=pass_send.at[group, dest - middle],
+            recv_sem=z_recv.at[group, 0],
+            device_id={"sp": dest},
+            device_id_type=MESH,
+        )
+
+    def pass_on(group):
+        kinds, which, which_seqs = groups_z[group]
+
+        @pl.when(z == 1)
+        def from_first():
+            view = heads.at[kinds, which_seqs, middle:z_count, pl.ds(0, half)]
+            pltpu.make_async_copy(view, view, z_recv.at[group, z_count]).wait()
+            for dest in right_dests:
+                pass_copy(group, dest).start()
 
     left_dests = tuple(range(middle))
     right_dests = tuple(range(z_count - 1, middle - 1, -1))
 
+    weights_landed(0)
     for number, (kind, low, high) in enumerate(pieces[:-1]):
+        if number + 1 < len(shared):
+            weights_landed(number + 1)
+        if number + 2 < len(pieces):
+            in_sib[number + 2].start()
+        if number >= len(shared):
+            weights_landed(number)
         weights_ready(number)
 
         def own_step(s, carry, kind=kind, low=low, high=high):
@@ -489,10 +555,13 @@
 
         lax.fori_loop(0, seqs, own_step, 0)
         each_send(kind, left_dests if low == 0 else right_dests, lambda copy: copy.start())
-
-    for s in range(seqs):
+        if kind > KEY and low > 0:
+            pass_on(kind - 1)
+
+    def other_rows(s):
         tok_x[s].wait_recv()
         normalize(s, 1)
+        each_border(s, lambda copy: copy.start())
         for group, kinds in ((3 + 2 * s, (KEY, VALUE)), (4 + 2 * s, (QUERY,))):
 
             def other_step(kind, carry, s=s):
@@ -503,26 +572,31 @@
             each_send(group, left_dests, lambda copy: copy.start())
             each_send(group, right_dests, lambda copy: copy.start())
 
-    weights_ready(len(pieces) - 1)
-    for s in range(seqs):
+    @pl.when(z == 0)
+    def no_border():
+        extended[:, 0:edge] = jnp.zeros((seqs, edge, cols), jnp.float32)
+
+    def take_border(s):
+        @pl.when(z > 0)
+        def take():
+            border_copy(s, 0).wait_recv()
+            extended[s, 0:edge] = project(border[s], POOL).astype(jnp.float32)
+
+    groups = cols // GROUP_WIDTH
+    own_lanes = pl.ds(pl.multiple_of(x * cols, cols), cols)
+    pool_copies = [
+        remote(
+            pool_tmp.at[s, pl.ds(pl.multiple_of(other_x * half, half), half)],
+            pool_rows.at[s, :, own_lanes],
+            {"tp": other_x},
+        )
+        for s in range(seqs)
+    ]
+
+    def pool_branch_rows(s):
         for which, owner in ((0, x), (1, other_x)):
             at = pl.multiple_of(edge + owner * half, edge)
             extended[s, pl.ds(at, half)] = project(rows_ref[s, which], POOL).astype(jnp.float32)
-
-    @pl.when(z > 0)
-    def take_border():
-        border_copy(0).wait_recv()
-        for s in range(seqs):
-            values = normalized(border[s])
-            extended[s, 0:edge] = project(values, POOL).astype(jnp.float32)
-
-    @pl.when(z == 0)
-    def no_border():
-        extended[:, 0:edge] = jnp.zeros((seqs, edge, cols), jnp.float32)
-
-    groups = cols // GROUP_WIDTH
-    pool_copies = []
-    for s in range(seqs):
         seen = (
             z * block + lax.broadcasted_iota(jnp.int32, (block, GROUP_WIDTH), 0) + 1
         ).astype(jnp.float32)
@@ -536,33 +610,22 @@
             departure = (averaged - plain[edge:]).astype(jnp.bfloat16)
             mixed = jnp.dot(departure, mix[x * groups + g], preferred_element_type=jnp.float32)
             pool_tmp[s, :, at] = (mixed * scale[x * groups + g]).astype(jnp.bfloat16)
-        lanes = pl.ds(pl.multiple_of(x * cols, cols), cols)
-        pool_rows[s, :, lanes] = pool_tmp[s, pl.ds(pl.multiple_of(x * half, half), half)]
-        copy = remote(
-            pool_tmp.at[s, pl.ds(pl.multiple_of(other_x * half, half), half)],
-            pool_rows.at[s, :, lanes],
-            {"tp": other_x},
-        )
-        copy.start()
-        pool_copies.append(copy)
-
-    arrive(out_x)
-    start(out_xy)
-    start(out_xs)
-    arrive(out_y)
-    start(out_ys)
-
+        pool_rows[s, :, own_lanes] = pool_tmp[s, pl.ds(pl.multiple_of(x * half, half), half)]
+        pool_copies[s].start()
 
     def head_lanes(owner_x, head):
         at = pl.multiple_of((owner_x * z_count + head) * HEAD_DIM, HEAD_DIM)
         return pl.ds(at, HEAD_DIM)
+
+    def attn_slot(index, head):
+        return head if index == 0 else z_count + head if index == 1 else 2 * z_count + index - 2
 
     def attn_copy(s, index, head, dest_x):
         first = index * block + dest_x * half
         return pltpu.make_async_remote_copy(
             src_ref=attn_own.at[s, head, first : first + half],
             dst_ref=attn_rows.at[s, :, head_lanes(x, head)],
-            send_sem=attn_send.at[s, index, head, dest_x],
+            send_sem=attn_send.at[s, attn_slot(index, head), dest_x],
             recv_sem=attn_recv.at[s, x * z_count + head],
             device_id={"sp": index, "tp": dest_x},
             device_id_type=MESH,
@@ -639,38 +702,82 @@
             return z, 1 + (z_count - 1) * z
         return z, z + 1
 
+    def first_rows(s):
+        pl.when(z == 0)(lambda: attention_rows(s, 0, *heads_of(0)))
+
+    def later_rows(s):
+        arriving = ((KEY, VALUE, QUERY) if s == 0 else ()) + (3 + 2 * s, 4 + 2 * s)
+        for group in arriving:
+            each_recv(group, range(middle))
+        pl.when(z < 2)(lambda: attention_rows(s, 1, *heads_of(1)))
+        if s == 0:
+            forward_half(0)
+        for index in range(middle, z_count):
+            for group in arriving:
+                each_recv(group, (index,))
+            attention_rows(s, index, *heads_of(index))
+
+    def forward_half(kind):
+        out_x[kind].wait_recv()
+        out_xy[kind].start()
+        out_xs[kind].start()
+
     for s in range(seqs):
-
-        @pl.when(z == 0)
-        def first_rows(s=s):
-            attention_rows(s, 0, *heads_of(0))
+        other_rows(s)
+        if s == 0:
+            start(out_sib)
+            weights_landed(len(pieces) - 1)
+            weights_ready(len(pieces) - 1)
+        take_border(s)
+        pool_branch_rows(s)
+        pass_on(3 + 2 * s)
+        first_rows(s)
 
     for s in range(seqs):
-        for group in ((KEY, VALUE, QUERY) if s == 0 else ()) + (3 + 2 * s, 4 + 2 * s):
-            each_recv(group)
-
-        @pl.when(z < 2)
-        def second_rows(s=s):
-            attention_rows(s, 1, *heads_of(1))
-
-        for index in range(2, z_count):
-            attention_rows(s, index, *heads_of(index))
-
+        later_rows(s)
+        if s == 0:
+            arrive(out_y)
+            start(out_ys)
+            forward_half(1)
+
+    for group in (tok_x, in_y, in_sib, in_corner, in_z, in_corner_other, out_x, out_y, out_sib):
+        for copy in group:
+            copy.wait_send()
+    for s in range(seqs):
+        each_border(s, lambda copy: copy.wait_send())
+
+    for group in range(len(groups_z)):
+        if not asks[group]:
+            for dest in right_dests:
+                pl.when(z == 1)(lambda group=group, dest=dest: pass_copy(group, dest).wait_send())
+        each_send(group, left_dests, lambda copy: copy.wait_send())
+        each_send(group, right_dests, lambda copy: copy.wait_send())
+    for copy in out_local:
+        copy.wait()
+
+    arrive(out_xy)
+    start(out_xys)
     arrive(out_xs)
     arrive(out_ys)
     arrive(out_sib)
-    arrive(out_xy)
-    start(out_xys)
-    for copy in out_local:
-        copy.wait()
-    arrive(out_xys)
-
-    def out_copy(s):
-        return pltpu.make_async_copy(out_stage.at[s], out.at[s], local_sem.at[s])
-
-    tile = min(512, width)
-
-    def output_step(s, carry):
+    arrive(pool_copies)
+
+    tiles = [f, sibling, across, f + 2 - 4 * (f // 2) + 1 - 2 * lax.rem(f, 2)]
+
+    def tile_lanes(tile):
+        return pl.ds(pl.multiple_of(tile * depth, depth), depth)
+
+    def pool_part(s, tile):
+        return jnp.dot(
+            pool_rows[s], w_out[0, :, tile_lanes(tile)], preferred_element_type=jnp.float32
+        )
+
+    def attn_part(s, tile):
+        return jnp.dot(
+            attn_rows[s], w_out[1, :, tile_lanes(tile)], preferred_element_type=jnp.float32
+        )
+
+    def attention_came(s):
         for source_x in range(2):
             for head in range(z_count):
                 made_here = (z == 0) | (z == head) | ((z == 1) & (head > 0))
@@ -681,36 +788,29 @@
                     number = source_x * z_count + head
                     pltpu.make_async_copy(view, view, attn_recv.at[s, number]).wait()
 
-        def tile_step(n, inner):
-            lanes = pl.ds(pl.multiple_of(n * tile, tile), tile)
-            result = jnp.dot(
-                pool_rows[s], w_out[0, :, lanes], preferred_element_type=jnp.float32
-            ) + jnp.dot(attn_rows[s], w_out[1, :, lanes], preferred_element_type=jnp.float32)
-            out_stage[s, :, lanes] = result.astype(jnp.bfloat16)
-            return inner
-
-        lax.fori_loop(0, width // tile, tile_step, 0)
-        out_copy(s).start()
-        return carry
-
-    arrive(pool_copies)
-    lax.fori_loop(0, seqs, output_step, 0)
+    for s in range(seqs - 1):
+        attention_came(s)
+        for number, tile in enumerate(tiles):
+            if s == 0 and number == len(tiles) - 1:
+                arrive(out_xys)
+            result = pool_part(s, tile) + attn_part(s, tile)
+            out[s, :, tile_lanes(tile)] = result.astype(jnp.bfloat16)
+    last = seqs - 1
+    if last == 0:
+        arrive(out_xys)
+    for tile in tiles:
+        pooled[:, tile_lanes(tile)] = pool_part(last, tile)
+    attention_came(last)
+    for tile in tiles:
+        result = pooled[:, tile_lanes(tile)] + attn_part(last, tile)
+        out[last, :, tile_lanes(tile)] = result.astype(jnp.bfloat16)
 
     for group in (
-        tok_x, in_y, in_sib, in_corner, out_x, out_y, out_sib, out_xy, out_xs, out_ys, out_xys,
+        out_xy, out_xs, out_ys, out_xys,
         pool_copies,
     ):
         for copy in group:
             copy.wait_send()
-
-    @pl.when(sends_border)
-    def border_sent():
-        for dest_x in range(2):
-            border_copy(dest_x).wait_send()
-
-    for group in range(len(groups_z)):
-        each_send(group, left_dests, lambda copy: copy.wait_send())
-        each_send(group, right_dests, lambda copy: copy.wait_send())
 
     def attention_sent(s, index):
         def head_step(head, carry):
@@ -729,7 +829,6 @@
         pl.when(z < 2)(lambda s=s: attention_sent(s, 1))
         for index in range(2, z_count):
             attention_sent(s, index)
-        out_copy(s).wait()
 
 
 def fast_device(
@@ -757,22 +856,14 @@
     dma = pltpu.SemaphoreType.DMA
     return pl.pallas_call(
         layer_kernel,
-        in_specs=[
-            anywhere,
-            inside,
-            anywhere,
-            inside,
-            inside,
-            anywhere,
-            anywhere,
-            anywhere,
-            inside,
-            anywhere,
-            anywhere,
-        ],
-        out_specs=anywhere,
-        out_shape=jax.ShapeDtypeStruct(tokens.shape, bf16),
+        in_specs=[anywhere] * 11,
+        out_specs=inside,
+        out_shape=pltpu.VMEM(tokens.shape, bf16),
         scratch_shapes=[
+            pltpu.VMEM((1, width), jnp.float32),
+            pltpu.VMEM(pool_mix.shape, bf16),
+            pltpu.VMEM((pool_mix.shape[0], 1, GROUP_WIDTH), jnp.float32),
+            pltpu.VMEM(gate_cache.shape, jnp.float32),
             pltpu.VMEM((4, width, cols), bf16),
             pltpu.VMEM((2, 2 * cols, width), bf16),
             pltpu.VMEM((seqs, 2, half, width), bf16),
@@ -783,19 +874,21 @@
             pltpu.VMEM((seqs, half, 2 * cols), bf16),
             pltpu.VMEM((seqs, z_count, length, HEAD_DIM), bf16),
             pltpu.VMEM((seqs, half, 2 * cols), bf16),
-            pltpu.VMEM((seqs, half, width), bf16),
-            dma((16,)),
-            dma((64,)),
-            dma((64,)),
+            pltpu.VMEM((half, width), jnp.float32),
+            dma((13 + seqs,)),
+            dma((39 + 2 * seqs,)),
+            dma((39 + 2 * seqs,)),
             dma((3 + 2 * seqs, z_count + 1)),
             dma((3 + 2 * seqs, z_count + 1)),
-            dma((seqs, z_count, z_count, 2)),
+            dma((seqs, 2 * z_count + 2, 2)),
             dma((seqs, 2 * z_count)),
+            dma((2, seqs)),
+            dma((3 + 2 * seqs, z_count // 2)),
         ],
         compiler_params=pltpu.CompilerParams(
             collective_id=0,
             has_side_effects=True,
-            vmem_limit_bytes=60 * 1024 * 1024,
+            vmem_limit_bytes=54 * 1024 * 1024,
         ),
     )(
         tokens,

time: 117 us -> 107 us (0.915)
  Pallas kernels: 113 us -> 106 us
  local copies, waits for them, and re-layouts: 3.16 us -> 1.32 us
    pallas_call x1, Pallas kernels: 113 us -> 106 us  [fast_device(): pl.pallas_call(layer_kernel, in_specs=[anywhere] * 11, out_specs=inside,...]
    unnamed x1, local copies, waits for them, and re-layouts: 3.16 us -> 1.32 us
where the time goes in v2:
time: 107 us
  Pallas kernels  106 us (99%)
  local copies, waits for them, and re-layouts  1.32 us (1%)
    pallas_call x1, Pallas kernels, fast_device(): pl.pallas_call(layer_kernel, in_specs=[anywhere] * 11, out_specs=inside,...  106 us

profile of v2, /device:TPU:27, one launch (start us, length us, event | category | flops | bytes accessed | tf_op | source)
XLA Modules:
  0.0 107.0 jit_solution(4710003568275532796)
XLA Ops:
  0.0 105.7 %shard_map.109 = bf16[2,256,2048]{2,1,0:T(8,128)(2,1)S(1)} custom-call(bf16[2,256,2048]{2,1,0:T(8,128)(2,1)} %tokens.1, f32[1,2048]{1,0:T(1,128)} %bitcast.2, bf16[512,512]{1,0:T(8,128)(2,1)} %w_pool.1, bf16[8,128,128]{2,1,0:T(8,128)(2,1)} %mix_in.1, f32[8,1,128]{2,1,0:T(1,128)} %bitcast.3, bf16[512,512]{1,0:T(8,128)(2,1)} %w_query.1, ...), custom_call_target="tpu_custom_call" | custom-call | tf_op jit(solution)/shard_map/pallas_call | solution.py:857
  105.7 1.3 %copy.13 = bf16[2,256,2048]{2,1,0:T(8,128)(2,1)} copy(bf16[2,256,2048]{2,1,0:T(8,128)(2,1)S(1)} %shard_map.109) | data formatting | bytes 4194304

commit v3 on v2

--- a/solution.py
+++ b/solution.py
@@ -470,16 +470,21 @@
         )
 
     def queries_go(dest):
-        return z >= 1 if dest == 0 else z >= z_count // 2
+        return z >= z_count // 2
 
     everything = pl.ds(0, seqs)
     groups_z = []
-    for kind in (KEY, VALUE, QUERY):
+    for kind in (KEY, VALUE):
         groups_z.append((pl.ds(kind, 1), 0, everything))
+    for s in range(seqs):
+        groups_z.append((pl.ds(QUERY, 1), 0, pl.ds(s, 1)))
     for s in range(seqs):
         groups_z.append((pl.ds(KEY, 2), 1, pl.ds(s, 1)))
         groups_z.append((pl.ds(QUERY, 1), 1, pl.ds(s, 1)))
-    asks = [g == QUERY or (g > QUERY and (g - QUERY) % 2 == 0) for g in range(len(groups_z))]
+    own_query = [2 + s for s in range(seqs)]
+    other_pair = [2 + seqs + 2 * s for s in range(seqs)]
+    other_query = [3 + seqs + 2 * s for s in range(seqs)]
+    asks = [g in own_query or g in other_query for g in range(len(groups_z))]
     middle = z_count // 2
 
     def each_send(group, dests, act):
@@ -488,7 +493,7 @@
             going = z != dest
             if asks[group]:
                 going = going & queries_go(dest)
-            elif dest >= middle:
+            else:
                 going = going & (z > 0)
 
             @pl.when(going)
@@ -499,14 +504,16 @@
 
             @pl.when(z == 0)
             def to_next():
-                act(z_copy(group, kinds, 1, which, which_seqs, middle, z_count))
+                act(z_copy(group, kinds, 1, which, which_seqs, 0, z_count))
 
     def each_recv(group, sources):
         kinds, which, which_seqs = groups_z[group]
         for source in sources:
+            if asks[group] and source < middle:
+                continue
             coming = z != source
-            if asks[group]:
-                coming = coming & ((z == 0) if source == 1 else (source >= middle))
+            if source == 0:
+                coming = coming & (z >= middle)
 
             @pl.when(coming)
             def came(source=source):
@@ -531,7 +538,7 @@
 
         @pl.when(z == 1)
         def from_first():
-            view = heads.at[kinds, which_seqs, middle:z_count, pl.ds(0, half)]
+            view = heads.at[kinds, which_seqs, 0:z_count, pl.ds(0, half)]
             pltpu.make_async_copy(view, view, z_recv.at[group, z_count]).wait()
             for dest in right_dests:
                 pass_copy(group, dest).start()
@@ -554,7 +561,8 @@
             return carry
 
         lax.fori_loop(0, seqs, own_step, 0)
-        each_send(kind, left_dests if low == 0 else right_dests, lambda copy: copy.start())
+        group = own_query[0] if kind == QUERY else kind
+        each_send(group, left_dests if low == 0 else right_dests, lambda copy: copy.start())
         if kind > KEY and low > 0:
             pass_on(kind - 1)
 
@@ -562,7 +570,7 @@
         tok_x[s].wait_recv()
         normalize(s, 1)
         each_border(s, lambda copy: copy.start())
-        for group, kinds in ((3 + 2 * s, (KEY, VALUE)), (4 + 2 * s, (QUERY,))):
+        for group, kinds in ((other_pair[s], (KEY, VALUE)), (other_query[s], (QUERY,))):
 
             def other_step(kind, carry, s=s):
                 project_heads(s, 1, kind, 0, cols)
@@ -674,13 +682,15 @@
             total = total + more_total
         attn_own[s, head, low:high] = (total / denominator).astype(jnp.bfloat16)
 
-    def attention_rows(s, index, first_head, last_head):
+    def attention_rows(s, index, first_head, last_head, later=False):
         def head_step(head, carry):
             attention_block(s, index, head)
             for dest_x in range(2):
                 here = (z == index) & (x == dest_x)
 
-                @pl.when(jnp.logical_not(here))
+                going = z != index if later else jnp.logical_not(here)
+
+                @pl.when(going)
                 def send(dest_x=dest_x):
                     attn_copy(s, index, head, dest_x).start()
 
@@ -699,22 +709,34 @@
         if index == 0:
             return 0, z_count
         if index == 1:
-            return z, 1 + (z_count - 1) * z
+            return 0, z_count
         return z, z + 1
 
     def first_rows(s):
-        pl.when(z == 0)(lambda: attention_rows(s, 0, *heads_of(0)))
+        later = 0 < s == seqs - 1
+        for index in range(2):
+            pl.when(z == index)(
+                lambda index=index: attention_rows(s, index, *heads_of(index), later=later)
+            )
+
+    def first_rows_across(s):
+        for index in range(2):
+            for dest_x in range(2):
+
+                @pl.when((z == index) & (x != dest_x))
+                def across_x(index=index, dest_x=dest_x):
+                    for head in range(z_count):
+                        attn_copy(s, index, head, dest_x).start()
 
     def later_rows(s):
-        arriving = ((KEY, VALUE, QUERY) if s == 0 else ()) + (3 + 2 * s, 4 + 2 * s)
+        arriving = ((KEY, VALUE) if s == 0 else ()) + (own_query[s], other_pair[s], other_query[s])
         for group in arriving:
             each_recv(group, range(middle))
-        pl.when(z < 2)(lambda: attention_rows(s, 1, *heads_of(1)))
-        if s == 0:
-            forward_half(0)
         for index in range(middle, z_count):
             for group in arriving:
                 each_recv(group, (index,))
+            if s == 0 and index == middle:
+                forward_half(1)
             attention_rows(s, index, *heads_of(index))
 
     def forward_half(kind):
@@ -724,22 +746,33 @@
 
     for s in range(seqs):
         other_rows(s)
+        if s + 1 < seqs:
+            each_send(own_query[s + 1], left_dests, lambda copy: copy.start())
+            each_send(own_query[s + 1], right_dests, lambda copy: copy.start())
         if s == 0:
             start(out_sib)
             weights_landed(len(pieces) - 1)
             weights_ready(len(pieces) - 1)
         take_border(s)
         pool_branch_rows(s)
-        pass_on(3 + 2 * s)
+        if s < seqs - 1:
+            pass_on(other_pair[s])
+    for s in range(seqs):
+        if s == seqs - 1:
+            forward_half(0)
+            pass_on(other_pair[s])
         first_rows(s)
 
     for s in range(seqs):
         later_rows(s)
+        if 0 < s == seqs - 1:
+            first_rows_across(s)
         if s == 0:
             arrive(out_y)
             start(out_ys)
-            forward_half(1)
-
+
+    out_xy[0].wait_recv()
+    out_xys[0].start()
     for group in (tok_x, in_y, in_sib, in_corner, in_z, in_corner_other, out_x, out_y, out_sib):
         for copy in group:
             copy.wait_send()
@@ -755,8 +788,8 @@
     for copy in out_local:
         copy.wait()
 
-    arrive(out_xy)
-    start(out_xys)
+    arrive(out_xy[1:])
+    start(out_xys[1:])
     arrive(out_xs)
     arrive(out_ys)
     arrive(out_sib)
@@ -777,32 +810,48 @@
             attn_rows[s], w_out[1, :, tile_lanes(tile)], preferred_element_type=jnp.float32
         )
 
+    def attn_side(s, tile, side):
+        at = pl.ds(pl.multiple_of(side * cols, cols), cols)
+        return jnp.dot(
+            attn_rows[s, :, at],
+            w_out[1, at, tile_lanes(tile)],
+            preferred_element_type=jnp.float32,
+        )
+
+    def own_side_came(s):
+        for head in range(z_count):
+
+            @pl.when(jnp.logical_not((z < 2) | (z == head)))
+            def came(head=head):
+                view = attn_rows.at[s, :, 0:HEAD_DIM]
+                pltpu.make_async_copy(view, view, attn_recv.at[s, x * z_count + head]).wait()
+
+    def other_side_came(s):
+        for head in range(z_count):
+            view = attn_rows.at[s, :, 0:HEAD_DIM]
+            pltpu.make_async_copy(view, view, attn_recv.at[s, other_x * z_count + head]).wait()
+
     def attention_came(s):
-        for source_x in range(2):
-            for head in range(z_count):
-                made_here = (z == 0) | (z == head) | ((z == 1) & (head > 0))
-
-                @pl.when(jnp.logical_not((x == source_x) & made_here))
-                def came(source_x=source_x, head=head):
-                    view = attn_rows.at[s, :, 0:HEAD_DIM]
-                    number = source_x * z_count + head
-                    pltpu.make_async_copy(view, view, attn_recv.at[s, number]).wait()
-
-    for s in range(seqs - 1):
-        attention_came(s)
+        own_side_came(s)
+        other_side_came(s)
+
+    for s in range(seqs):
         for number, tile in enumerate(tiles):
             if s == 0 and number == len(tiles) - 1:
                 arrive(out_xys)
-            result = pool_part(s, tile) + attn_part(s, tile)
+            pooled[s, :, tile_lanes(tile)] = pool_part(s, tile)
+    last = seqs - 1
+    for s in range(last):
+        attention_came(s)
+        for tile in tiles:
+            result = pooled[s, :, tile_lanes(tile)] + attn_part(s, tile)
             out[s, :, tile_lanes(tile)] = result.astype(jnp.bfloat16)
-    last = seqs - 1
-    if last == 0:
-        arrive(out_xys)
+    own_side_came(last)
     for tile in tiles:
-        pooled[:, tile_lanes(tile)] = pool_part(last, tile)
-    attention_came(last)
+        pooled[last, :, tile_lanes(tile)] += attn_side(last, tile, x)
+    other_side_came(last)
     for tile in tiles:
-        result = pooled[:, tile_lanes(tile)] + attn_part(last, tile)
+        result = pooled[last, :, tile_lanes(tile)] + attn_side(last, tile, other_x)
         out[last, :, tile_lanes(tile)] = result.astype(jnp.bfloat16)
 
     for group in (
@@ -826,7 +875,7 @@
 
     for s in range(seqs):
         pl.when(z == 0)(lambda s=s: attention_sent(s, 0))
-        pl.when(z < 2)(lambda s=s: attention_sent(s, 1))
+        pl.when(z == 1)(lambda s=s: attention_sent(s, 1))
         for index in range(2, z_count):
             attention_sent(s, index)
 
@@ -874,16 +923,16 @@
             pltpu.VMEM((seqs, half, 2 * cols), bf16),
             pltpu.VMEM((seqs, z_count, length, HEAD_DIM), bf16),
             pltpu.VMEM((seqs, half, 2 * cols), bf16),
-            pltpu.VMEM((half, width), jnp.float32),
+            pltpu.VMEM((seqs, half, width), jnp.float32),
             dma((13 + seqs,)),
             dma((39 + 2 * seqs,)),
             dma((39 + 2 * seqs,)),
-            dma((3 + 2 * seqs, z_count + 1)),
-            dma((3 + 2 * seqs, z_count + 1)),
+            dma((2 + 3 * seqs, z_count + 1)),
+            dma((2 + 3 * seqs, z_count + 1)),
             dma((seqs, 2 * z_count + 2, 2)),
             dma((seqs, 2 * z_count)),
             dma((2, seqs)),
-            dma((3 + 2 * seqs, z_count // 2)),
+            dma((2 + 3 * seqs, z_count // 2)),
         ],
         compiler_params=pltpu.CompilerParams(
             collective_id=0,

time: 107 us -> 104 us (0.972)
  Pallas kernels: 106 us -> 103 us
    pallas_call x1, Pallas kernels: 106 us -> 103 us  [fast_device(): pl.pallas_call(layer_kernel, in_specs=[anywhere] * 11, out_specs=inside,...]
where the time goes in v3:
time: 104 us
  Pallas kernels  103 us (99%)
  local copies, waits for them, and re-layouts  1.32 us (1%)
    pallas_call x1, Pallas kernels, fast_device(): pl.pallas_call(layer_kernel, in_specs=[anywhere] * 11, out_specs=inside,...  103 us

profile of v3, /device:TPU:27, one launch (start us, length us, event | category | flops | bytes accessed | tf_op | source)
XLA Modules:
  0.0 104.2 jit_solution(15897620129136793773)
XLA Ops:
  0.0 102.8 %shard_map.109 = bf16[2,256,2048]{2,1,0:T(8,128)(2,1)S(1)} custom-call(bf16[2,256,2048]{2,1,0:T(8,128)(2,1)} %tokens.1, f32[1,2048]{1,0:T(1,128)} %bitcast.2, bf16[512,512]{1,0:T(8,128)(2,1)} %w_pool.1, bf16[8,128,128]{2,1,0:T(8,128)(2,1)} %mix_in.1, f32[8,1,128]{2,1,0:T(1,128)} %bitcast.3, bf16[512,512]{1,0:T(8,128)(2,1)} %w_query.1, ...), custom_call_target="tpu_custom_call" | custom-call | tf_op jit(solution)/shard_map/pallas_call | solution.py:906
  102.8 1.3 %copy.13 = bf16[2,256,2048]{2,1,0:T(8,128)(2,1)} copy(bf16[2,256,2048]{2,1,0:T(8,128)(2,1)S(1)} %shard_map.109) | data formatting | bytes 4194304

commit v4 on v3

--- a/solution.py
+++ b/solution.py
@@ -732,6 +732,12 @@
         arriving = ((KEY, VALUE) if s == 0 else ()) + (own_query[s], other_pair[s], other_query[s])
         for group in arriving:
             each_recv(group, range(middle))
+        if 0 < s == seqs - 1:
+            for group in arriving:
+                each_recv(group, range(middle, z_count))
+            for index in range(z_count - 1, middle - 1, -1):
+                attention_rows(s, index, *heads_of(index))
+            return
         for index in range(middle, z_count):
             for group in arriving:
                 each_recv(group, (index,))

time: 104 us -> 105 us (level)
  the two profiles are of different devices: /device:TPU:27 before, /device:TPU:19 now
where the time goes in v4:
time: 105 us
  Pallas kernels  103 us (98%)
  local copies, waits for them, and re-layouts  1.32 us (1%)
    pallas_call x1, Pallas kernels, fast_device(): pl.pallas_call(layer_kernel, in_specs=[anywhere] * 11, out_specs=inside,...  103 us

profile of v4, /device:TPU:19, one launch (start us, length us, event | category | flops | bytes accessed | tf_op | source)
XLA Modules:
  0.0 104.6 jit_solution(12840943268700636810)
XLA Ops:
  0.0 103.3 %shard_map.109 = bf16[2,256,2048]{2,1,0:T(8,128)(2,1)S(1)} custom-call(bf16[2,256,2048]{2,1,0:T(8,128)(2,1)} %tokens.1, f32[1,2048]{1,0:T(1,128)} %bitcast.2, bf16[512,512]{1,0:T(8,128)(2,1)} %w_pool.1, bf16[8,128,128]{2,1,0:T(8,128)(2,1)} %mix_in.1, f32[8,1,128]{2,1,0:T(1,128)} %bitcast.3, bf16[512,512]{1,0:T(8,128)(2,1)} %w_query.1, ...), custom_call_target="tpu_custom_call" | custom-call | tf_op jit(solution)/shard_map/pallas_call | solution.py:912
  103.3 1.3 %copy.13 = bf16[2,256,2048]{2,1,0:T(8,128)(2,1)} copy(bf16[2,256,2048]{2,1,0:T(8,128)(2,1)S(1)} %shard_map.109) | data formatting | bytes 4194304
